TPU v7x, 512 devices: a whole 4x8x8 slice. The times are simulated.
512 devices in a mesh: sp: 32 (over z, x), tp: 16 (over y, core).
Axes of the slice: x: 4, y: 8, z: 8, core: 2. Of those that a mesh axis runs over, the one named last changes fastest.
Arguments:
- pool_input: bfloat16 [1024, 12288], P('tp', 'sp'), may hold values from -6 to 6
- pool_gate: bfloat16 [1024, 12288], P('tp', 'sp'), may hold values from -6 to 6
- pool_mix: bfloat16 [4, 256, 256], replicated, may hold values from -0.375 to 0.375
- pool_scale: float32 [1024], replicated, may hold values from 0.1 to 1.9
- out_proj: bfloat16 [1024, 2048], P(None, 'tp'), may hold values from -0.375 to 0.375
- residual: bfloat16 [12288, 2048], P('sp', 'tp'), may hold values from -12 to 12
- norm_gain: float32 [2048], P('tp'), may hold values from 0.1 to 1.9
- routes: int32 [12288, 2], P('sp'), may hold values from 0 to 31, all different within a row; in each aligned block of 384 rows (0 to 383, 384 to 767, ...) at most 36 rows name the same one
- group_logits: float32 [12288, 4], P('sp'), may hold values from -4 to 4
- expert_scores: float32 [12288, 2], P('sp'), may hold values from -4 to 4
- w_gate: bfloat16 [32, 2048, 4096], P('sp', None, 'tp'), may hold values from -0.125 to 0.125
- w_up: bfloat16 [32, 2048, 4096], P('sp', None, 'tp'), may hold values from -0.125 to 0.125
- w_down: bfloat16 [32, 4096, 2048], P('sp', None, 'tp'), may hold values from -0.375 to 0.375
Outputs:
- layer_out: bfloat16 [12288, 2048], P('sp', 'tp')
Inputs may be any that keep to these rules, and one draw needn't show every extreme that they name: `routes`: among the rows of one device (aligned blocks of 384 rows) no expert is named by more than 36 rows, a bound that some block reaches; the 2 experts of a row differ.
All inputs are finite; a program needn't handle non-finite values.
Results may differ from a plain program's by a relative error of at most 0.01.
Values may be sent and summed in bfloat16 or wider, within the bound.
No kernel may reach another device: no remote copies, remote signals or barrier semaphores. Data moves between devices by JAX's collectives and lax.ppermute only.
A program may use at most 64 MiB of HBM per device.

v0:
```python
import jax
import jax.numpy as jnp
from jax import lax
from jax.sharding import PartitionSpec as P

D = 2048
POOL_GROUP = 256
TOP = 2
reach_back = 15
epsilon = 1e-06


def from_behind(value, axis, steps):
    count = lax.axis_size(axis)
    initial, last = (max(0, -steps), min(count, count - steps))
    return lax.ppermute(value, axis, [(source, source + steps) for source in range(initial, last)])


def in_one_piece(arrays, axis, dim, along):
    ends, at = ([], 0)
    for a in arrays[:-1]:
        at += a.shape[along]
        ends.append(at)
    both = jnp.concatenate(arrays, axis=along)
    return tuple(jnp.split(lax.all_gather(both, axis, axis=dim, tiled=True), ends, axis=along))


def from_everyone(value, axis):
    count = lax.axis_size(axis)
    return lax.all_to_all(
        jnp.broadcast_to(value[None], (count, *value.shape)), axis, 0, 0, tiled=True
    )


def over_copies(value, axis):
    return from_everyone(value, axis).sum(axis=0)


def window_terms(extended, first_channel, first_position, group_width):
    length = extended.shape[1] - reach_back
    layered = extended
    stride = 1
    partial_sums = []
    for _ in range(4):
        layered = layered[:, stride:] + layered[:, :-stride]
        stride = stride * 2
        partial_sums.append(layered[:, layered.shape[1] - length :])
    channel = first_channel + jnp.arange(extended.shape[0], dtype=jnp.int32)
    scale_index = channel // group_width
    chosen = partial_sums[3]
    for octave in range(3):
        chosen = jnp.where((scale_index == octave)[:, None], partial_sums[octave], chosen)
    window = (2 ** (scale_index + 1)).astype(jnp.float32)
    positions = (first_position + jnp.arange(length, dtype=jnp.int32) + 1).astype(jnp.float32)
    counted = jnp.minimum(positions[None, :], window[:, None])
    return chosen / counted - extended[:, reach_back:]


def slot_table(row_block, experts, capacity):
    flattened = row_block.reshape(-1)
    onehot = (flattened[:, None] == jnp.arange(experts, dtype=jnp.int32)[None, :]).astype(jnp.int32)
    before = jnp.cumsum(onehot, axis=0) - onehot
    ranked = jnp.sum(before * onehot, axis=1)
    return flattened * capacity + ranked


def route_weights(routes, group_logits, expert_scores, per_group):
    raised = jnp.exp(group_logits)
    group_prob = raised / jnp.sum(raised, axis=1, keepdims=True)
    owning_group = routes // per_group
    groups_iota = jnp.arange(group_logits.shape[1], dtype=jnp.int32)
    picked = jnp.sum(
        jnp.where(
            owning_group[:, :, None] == groups_iota[None, None, :], group_prob[:, None, :], 0.0
        ),
        axis=2,
    )
    lifted = jnp.exp(expert_scores)
    return picked * lifted / jnp.sum(lifted, axis=1, keepdims=True)


def per_device(
    pool_input,
    pool_gate,
    pool_mix,
    pool_scale,
    out_proj,
    residual,
    norm_gain,
    routes,
    group_logits,
    expert_scores,
    w_gate,
    w_up,
    w_down,
):
    channels, length = pool_input.shape
    edge_rows = from_behind(pool_input[:, length - reach_back :], "sp", 1)
    extended = jnp.concatenate([edge_rows, pool_input], axis=1).astype(jnp.float32)
    first_channel = lax.axis_index("tp") * channels
    first_position = lax.axis_index("sp") * length
    pooled = window_terms(extended, first_channel, first_position, POOL_GROUP).astype(jnp.bfloat16)
    gathered, gate_rows = in_one_piece((pooled, pool_gate), "tp", 0, 1)
    scales = pool_mix.shape[0]
    mixed_rows = jnp.einsum(
        "gct,gcd->tgd",
        gathered.reshape(scales, POOL_GROUP, length),
        pool_mix,
        preferred_element_type=jnp.float32,
    ).reshape(length, scales * POOL_GROUP)
    branch = (
        jax.nn.sigmoid(gate_rows.T.astype(jnp.float32)) * mixed_rows * pool_scale[None, :]
    ).astype(jnp.bfloat16)
    hidden_state = (
        residual.astype(jnp.float32) + jnp.dot(branch, out_proj, preferred_element_type=jnp.float32)
    ).astype(jnp.bfloat16)
    state_float = hidden_state.astype(jnp.float32)
    squares = over_copies(jnp.sum(state_float * state_float, axis=1), "tp")
    normed = (state_float * lax.rsqrt(squares / D + epsilon)[:, None] * norm_gain[None, :]).astype(
        jnp.bfloat16
    )
    experts = lax.axis_size("sp") * w_gate.shape[0]
    weights = route_weights(routes, group_logits, expert_scores, experts // group_logits.shape[1])
    capacity = 3 * TOP * length // (2 * experts)
    destination = slot_table(routes, experts, capacity)
    token_index = jnp.arange(length * TOP, dtype=jnp.int32) // TOP
    sources = jnp.full((experts * capacity,), length, jnp.int32).at[destination].set(token_index)
    padded = jnp.concatenate([normed, jnp.zeros((1, normed.shape[1]), jnp.bfloat16)], axis=0)
    arrived = lax.all_to_all(padded[sources], "sp", split_axis=0, concat_axis=0, tiled=True)
    portion = lax.all_gather(arrived, "tp", axis=1, tiled=True)
    rows_gate = w_gate[0]
    rows_up = w_up[0]
    gate_term = jnp.dot(portion, rows_gate, preferred_element_type=jnp.float32)
    up_term = jnp.dot(portion, rows_up, preferred_element_type=jnp.float32)
    activated = (jax.nn.silu(gate_term) * up_term).astype(jnp.bfloat16)
    rows_down = w_down[0]
    result = jnp.dot(
        lax.all_gather(activated, "tp", axis=1, tiled=True),
        rows_down,
        preferred_element_type=jnp.float32,
    ).astype(jnp.bfloat16)
    returned = lax.all_to_all(result, "sp", split_axis=0, concat_axis=0, tiled=True)
    picked = returned[destination].astype(jnp.float32).reshape(length, TOP, returned.shape[1])
    combined = jnp.sum(weights[:, :, None] * picked, axis=1)
    return (state_float + combined).astype(jnp.bfloat16)


def solution(mesh):
    placed = (
        P("tp", "sp"),
        P("tp", "sp"),
        P(),
        P(),
        P(None, "tp"),
        P("sp", "tp"),
        P("tp"),
        P("sp", None),
        P("sp", None),
        P("sp", None),
        P("sp", None, "tp"),
        P("sp", None, "tp"),
        P("sp", None, "tp"),
    )
    return jax.shard_map(
        per_device, mesh=mesh, in_specs=placed, out_specs=P("sp", "tp"), check_vma=False
    )
```

profile of v0, /device:TPU:16, one launch (start us, length us, event | category | flops | bytes accessed | tf_op | source)
XLA Modules:
  0.0 268.7 jit_solution(10977367310961019468)
XLA Ops:
  6.5 0.9 slice.43
  7.4 3.4 %collective-permute-start = (bf16[64,15]{1,0:T(8,128)(2,1)S(1)}, bf16[64,15]{1,0:T(8,128)(2,1)S(1)}, u32[]{:S(2)}, u32[]{:S(2)}) collective-permute-start(bf16[64,15]{1,0:T(8,128)(2,1)S(1)} %slice.43), channel_id=1, source_target_pairs={{0,16},{16,32},{32,48},{48,64},{64,80},{80,96},{96,112},{112,128},... | collective-permute-start | bytes 5768 | tf_op jit(solution)/shard_map/ppermute | solution.py:16
  10.9 1.3 collective-permute-done
  12.2 0.9 maximum_convert_fusion
  13.7 0.7 pad_maximum_fusion
  14.8 1.7 reduce-window.6
  17.3 3.4 %scatter_custom_fusion = s32[1152]{0:T(1024)S(1)} fusion(s32[768]{0:T(1024)S(1)} %fusion.24, s32[768]{0:T(1024)S(1)} %add_select_fusion, s32[]{:T(128)} %constant.90.clone.1), kind=kCustom, calls=%fused_computation.60 | custom fusion | bytes 4612 | tf_op jit(solution)/shard_map/scatter | solution.py:127
  20.7 39.9 %all-gather.4.cloned.1.call-done = bf16[1024,768]{1,0:T(8,128)(2,1)} async-done(((bf16[64,768]{1,0:T(8,128)(2,1)}), bf16[1024,768]{1,0:T(8,128)(2,1)}) %all-gather.4.cloned.1.call-update) | async-done | bytes 1572880 | tf_op jit(solution)/shard_map/all_gather | solution.py:25
  60.7 1.6 slice-done
  64.9 6.4 %all-to-all-start = ((f32[16,1,384]{2,1,0:T(1,128)}), f32[16,1,384]{2,1,0:T(1,128)S(1)}, u32[]{:S(2)}, u32[]{:S(2)}) async-start(f32[16,1,384]{2,1,0:T(1,128)} %broadcast_in_dim.69), calls=%async_computation | async-start | bytes 49152 | tf_op jit(solution)/shard_map/all_to_all | solution.py:30
  71.3 5.4 %all-to-all-done = f32[16,1,384]{2,1,0:T(1,128)S(1)} async-done(((f32[16,1,384]{2,1,0:T(1,128)}), f32[16,1,384]{2,1,0:T(1,128)S(1)}, u32[]{:S(2)}, u32[]{:S(2)}) %all-to-all-start) | async-done | bytes 24608 | tf_op jit(solution)/shard_map/all_to_all | solution.py:30
  76.9 2.9 %gather_fusion = bf16[1152,128]{1,0:T(8,128)(2,1)S(1)} fusion(bf16[385,128]{1,0:T(8,128)(2,1)S(1)} %concatenate.11, s32[2048]{0:T(1024)S(1)} %pad_clamp_fusion), kind=kCustom, calls=%fused_computation | custom fusion | bytes 594432 | tf_op jit(solution)/shard_map/gather | solution.py:129
  79.9 24.5 %all_to_all.30 = bf16[32,36,128]{2,1,0:T(8,128)(2,1)S(1)} all-to-all(bf16[32,36,128]{2,1,0:T(8,128)(2,1)S(1)} %all_to_all.21), channel_id=1, replica_groups=mesh['sp'=32,'tp'=16] {'sp'}, dimensions={0} | all-to-all | bytes 589824 | tf_op jit(solution)/shard_map/all_to_all | solution.py:129
  104.4 0.8 all_to_all.23
  105.2 45.1 %all-gather.6.cloned.1.call-done = bf16[1152,2048]{1,0:T(8,128)(2,1)} async-done(((bf16[1152,128]{1,0:T(8,128)(2,1)}), bf16[1152,2048]{1,0:T(8,128)(2,1)}) %all-gather.6.cloned.1.call-update) | async-done | bytes 4718608 | tf_op jit(solution)/shard_map/all_gather | solution.py:130
  150.3 3.9 %fusion.7 = f32[1152,256]{1,0:T(8,128)S(1)} fusion(bf16[1152,2048]{1,0:T(8,128)(2,1)} %all-gather.6.cloned.1.call-done, bf16[1,2048,256]{2,1,0:T(8,128)(2,1)S(1)} %copy-done), kind=kOutput, calls=%fused_computation.14 | convolution fusion | flops 1207959552 | bytes 6946816 | tf_op jit(solution)/shard_map/dot_general | solution.py:133
  154.2 2.3 fusion
  156.7 71.4 %all-gather.8.cloned.1.call-done = bf16[1152,4096]{1,0:T(8,128)(2,1)} async-done(((bf16[1152,256]{1,0:T(8,128)(2,1)}), bf16[1152,4096]{1,0:T(8,128)(2,1)}) %all-gather.8.cloned.1.call-update) | async-done | bytes 9437200 | tf_op jit(solution)/shard_map/all_gather | solution.py:138
  228.1 6.5 %convolution_convert_fusion = bf16[1152,128]{1,0:T(8,128)(2,1)S(1)} fusion(bf16[1152,4096]{1,0:T(8,128)(2,1)} %all-gather.8.cloned.1.call-done, bf16[1,4096,128]{2,1,0:T(8,128)(2,1)} %param.25), kind=kOutput, calls=%fused_computation.5 | convolution fusion | flops 1208107008 | bytes 10780672 | tf_op jit(solution)/shard_map/dot_general | solution.py:137
  234.6 0.8 all_to_all.24
  235.3 9.0 %all-to-all-start.2 = ((bf16[32,36,128]{2,1,0:T(8,128)(2,1)}), bf16[32,36,128]{2,1,0:T(8,128)(2,1)S(1)}, u32[]{:S(2)}, u32[]{:S(2)}) async-start(bf16[32,36,128]{2,1,0:T(8,128)(2,1)} %all_to_all.24), calls=%async_computation.2 | async-start | bytes 655360 | tf_op jit(solution)/shard_map/all_to_all | solution.py:142
  244.6 14.4 %all-to-all-done.2 = bf16[32,36,128]{2,1,0:T(8,128)(2,1)S(1)} async-done(((bf16[32,36,128]{2,1,0:T(8,128)(2,1)}), bf16[32,36,128]{2,1,0:T(8,128)(2,1)S(1)}, u32[]{:S(2)}, u32[]{:S(2)}) %all-to-all-start.2) | async-done | bytes 294944 | tf_op jit(solution)/shard_map/all_to_all | solution.py:142
  259.0 1.9 gather_fusion.1
  261.5 0.7 add_convert_fusion
  (73 shorter events, 5.6 us)
Async XLA Ops:
  6.5 143.8 %copy-start = (bf16[1,2048,256]{2,1,0:T(8,128)(2,1)S(1)}, bf16[1,2048,256]{2,1,0:T(8,128)(2,1)}, u32[]{:S(2)}) copy-start(bf16[1,2048,256]{2,1,0:T(8,128)(2,1)} %param.23) | copy-start | bytes 3145732
  6.5 7.1 %copy-start.5 = (bf16[64,384]{1,0:T(8,128)(2,1)S(1)}, bf16[64,384]{1,0:T(8,128)(2,1)}, u32[]{:S(2)}) copy-start(bf16[64,384]{1,0:T(8,128)(2,1)} %param.14) | copy-start | bytes 147460
  6.5 7.8 %copy-start.8 = (s32[384,2]{0,1:T(2,128)S(1)}, s32[384,2]{0,1:T(2,128)}, u32[]{:S(2)}) copy-start(s32[384,2]{0,1:T(2,128)} %param.20) | copy-start | bytes 9220
  6.5 54.1 %all-gather.4.cloned.1.call-start = ((), (), s32[]{:S(2)}) async-start(), calls=%async_computation.3 | async-start | bytes 1671168 | tf_op jit(solution)/shard_map/all_gather | solution.py:25
  7.4 4.8 %collective-permute-start = (bf16[64,15]{1,0:T(8,128)(2,1)S(1)}, bf16[64,15]{1,0:T(8,128)(2,1)S(1)}, u32[]{:S(2)}, u32[]{:S(2)}) collective-permute-start(bf16[64,15]{1,0:T(8,128)(2,1)S(1)} %slice.43), channel_id=1, source_target_pairs={{0,16},{16,32},{32,48},{48,64},{64,80},{80,96},{96,112},{112,128},... | collective-permute-start | bytes 5768 | tf_op jit(solution)/shard_map/ppermute | solution.py:16
  14.4 46.3 %copy-start.2 = (bf16[4,256,256]{2,1,0:T(8,128)(2,1)S(1)}, bf16[4,256,256]{2,1,0:T(8,128)(2,1)}, u32[]{:S(2)}) copy-start(bf16[4,256,256]{2,1,0:T(8,128)(2,1)} %param.15) | copy-start | bytes 1572868
  60.6 1.6 slice-start
  60.7 2.1 copy-start.1
  60.7 2.1 copy-start.9
  62.8 1.0 copy-start.3
  62.8 1.0 copy-start.4
  62.8 13.9 %copy-start.10 = (f32[128]{0:T(128)S(1)}, f32[128]{0:T(128)}, u32[]{:S(2)}) copy-start(f32[128]{0:T(128)} %param.19) | copy-start | bytes 1540
  64.9 11.8 %all-to-all-start = ((f32[16,1,384]{2,1,0:T(1,128)}), f32[16,1,384]{2,1,0:T(1,128)S(1)}, u32[]{:S(2)}, u32[]{:S(2)}) async-start(f32[16,1,384]{2,1,0:T(1,128)} %broadcast_in_dim.69), calls=%async_computation | async-start | bytes 49152 | tf_op jit(solution)/shard_map/all_to_all | solution.py:30
  71.3 79.0 %all-gather.6.cloned.1.call-start = ((), (), s32[]{:S(2)}) async-start(), calls=%async_computation.4 | async-start | bytes 5013504 | tf_op jit(solution)/shard_map/all_gather | solution.py:130
  105.2 49.0 %copy-start.12 = (bf16[1,2048,256]{2,1,0:T(8,128)(2,1)S(1)}, bf16[1,2048,256]{2,1,0:T(8,128)(2,1)}, u32[]{:S(2)}) copy-start(bf16[1,2048,256]{2,1,0:T(8,128)(2,1)} %param.24) | copy-start | bytes 3145732
  105.2 122.9 %all-gather.8.cloned.1.call-start = ((), (), s32[]{:S(2)}) async-start(), calls=%async_computation.5 | async-start | bytes 10027008 | tf_op jit(solution)/shard_map/all_gather | solution.py:138
  150.3 3.9 %copy-start.11 = (bf16[1152,2048]{1,0:T(8,128)(2,1)S(1)}, bf16[1152,2048]{1,0:T(8,128)(2,1)}, u32[]{:S(2)}) copy-start(bf16[1152,2048]{1,0:T(8,128)(2,1)} %all-gather.6.cloned.1.call-done) | copy-start | bytes 14155780
  154.2 2.4 copy-start.6
  156.7 87.7 %copy-start.7 = (f32[384,2]{0,1:T(2,128)S(1)}, f32[384,2]{0,1:T(2,128)}, u32[]{:S(2)}) copy-start(f32[384,2]{0,1:T(2,128)} %param.22) | copy-start | bytes 9220
  235.3 23.6 %all-to-all-start.2 = ((bf16[32,36,128]{2,1,0:T(8,128)(2,1)}), bf16[32,36,128]{2,1,0:T(8,128)(2,1)S(1)}, u32[]{:S(2)}, u32[]{:S(2)}) async-start(bf16[32,36,128]{2,1,0:T(8,128)(2,1)} %all_to_all.24), calls=%async_computation.2 | async-start | bytes 655360 | tf_op jit(solution)/shard_map/all_to_all | solution.py:142
Sparse Core Ops, SparseCore 0:
  14.5 46.1 all-gather.3
  105.3 44.9 all-gather.5
  156.7 71.2 all-gather.7
where the time goes:
time: 269 us
  waiting for transfers between devices  178 us (66%)
  blocking collectives  24.5 us (9%)
  starting transfers between devices  18.8 us (7%)
  local copies, waits for them, and re-layouts  14.7 us (5%)
  matrix products  13.7 us (5%)
  between operations  13.5 us (5%)
  other arithmetic  5.95 us (2%)
    all_gather x1, waiting for transfers between devices, per_device(): lax.all_gather(activated, 'tp', axis=1, tiled=True)  71.4 us
    all_gather x1, waiting for transfers between devices, per_device(): portion = lax.all_gather(arrived, 'tp', axis=1, tiled=True)  45.1 us
    all_gather x1, waiting for transfers between devices, in_one_piece(): lax.all_gather(both, axis, axis=dim, tiled=True)  39.9 us
    all_to_all x1, blocking collectives, per_device(): lax.all_to_all(padded[sources], 'sp', split_axis=0, concat_axis=0, tiled=...  24.5 us
    all_to_all x1, waiting for transfers between devices, per_device(): lax.all_to_all(result, 'sp', split_axis=0, concat_axis=0, tiled=True)  14.4 us
    all_to_all x1, starting transfers between devices, per_device(): lax.all_to_all(result, 'sp', split_axis=0, concat_axis=0, tiled=True)  8.98 us
    dot_general x1, matrix products, per_device(): jnp.dot(lax.all_gather(activated, 'tp', axis=1, tiled=True), rows_down, p...  6.52 us
    all_to_all x1, starting transfers between devices, from_everyone(): lax.all_to_all(jnp.broadcast_to(value[None], (count, *value.shape)), axis...  6.36 us
  transfers between devices with their start and end apart: 6, of which 6 were waited for; matrix products, arithmetic and copies ran while one was open for 2% of the time, Pallas kernels for 0%

commit v1 on v0

--- a/solution.py
+++ b/solution.py
@@ -134,10 +134,20 @@
     up_term = jnp.dot(portion, rows_up, preferred_element_type=jnp.float32)
     activated = (jax.nn.silu(gate_term) * up_term).astype(jnp.bfloat16)
     rows_down = w_down[0]
+
+    def treat_the_object(local):
+        return jnp.concatenate(
+            jax.lax.all_to_all(
+                jnp.stack(jax.lax.axis_size("tp") * [local], 0),
+                concat_axis=0,
+                axis_name="tp",
+                split_axis=0,
+            ),
+            1,
+        )
+
     result = jnp.dot(
-        lax.all_gather(activated, "tp", axis=1, tiled=True),
-        rows_down,
-        preferred_element_type=jnp.float32,
+        treat_the_object(activated), rows_down, preferred_element_type=jnp.float32
     ).astype(jnp.bfloat16)
     returned = lax.all_to_all(result, "sp", split_axis=0, concat_axis=0, tiled=True)
     picked = returned[destination].astype(jnp.float32).reshape(length, TOP, returned.shape[1])

time: 269 us -> 415 us (1.54)
  the two profiles are of different devices: /device:TPU:16 before, /device:TPU:24 now
where the time goes in v1:
time: 415 us
  waiting for transfers between devices  313 us (75%)
  starting transfers between devices  25 us (6%)
  blocking collectives  24.5 us (6%)
  local copies, waits for them, and re-layouts  19.9 us (5%)
  between operations  13.8 us (3%)
  matrix products  12.8 us (3%)
  other arithmetic  5.95 us (1%)
    all_to_all x1, waiting for transfers between devices, treat_the_object(): jax.lax.all_to_all(jnp.stack(jax.lax.axis_size('tp') * [local], 0), conca...  206 us
    all_gather x1, waiting for transfers between devices, per_device(): portion = lax.all_gather(arrived, 'tp', axis=1, tiled=True)  45.8 us
    all_gather x1, waiting for transfers between devices, in_one_piece(): lax.all_gather(both, axis, axis=dim, tiled=True)  41 us
    all_to_all x1, blocking collectives, per_device(): lax.all_to_all(padded[sources], 'sp', split_axis=0, concat_axis=0, tiled=...  24.5 us
    all_to_all x1, waiting for transfers between devices, per_device(): lax.all_to_all(result, 'sp', split_axis=0, concat_axis=0, tiled=True)  14.2 us
    all_to_all x1, starting transfers between devices, per_device(): lax.all_to_all(result, 'sp', split_axis=0, concat_axis=0, tiled=True)  9.07 us
  transfers between devices with their start and end apart: 6, of which 6 were waited for; matrix products, arithmetic and copies ran while one was open for 2% of the time, Pallas kernels for 0%

profile of v1, /device:TPU:24, one launch (start us, length us, event | category | flops | bytes accessed | tf_op | source)
XLA Modules:
  0.0 414.9 jit_solution(18234477456770079069)
XLA Ops:
  6.5 0.9 slice.43
  7.4 3.4 collective-permute-start
  10.9 1.3 collective-permute-done
  12.2 0.9 maximum_convert_fusion
  14.8 1.7 reduce-window.6
  17.3 3.4 scatter_custom_fusion
  20.7 41.0 %all-gather.3.cloned.1.call-done = bf16[1024,768]{1,0:T(8,128)(2,1)} async-done(((bf16[64,768]{1,0:T(8,128)(2,1)}), bf16[1024,768]{1,0:T(8,128)(2,1)}) %all-gather.3.cloned.1.call-update) | async-done | bytes 1572880 | tf_op jit(solution)/shard_map/all_gather | solution.py:25
  61.8 1.6 slice-done
  66.0 5.1 %all-to-all-start = ((f32[16,1,384]{2,1,0:T(1,128)}), f32[16,1,384]{2,1,0:T(1,128)S(1)}, u32[]{:S(2)}, u32[]{:S(2)}) async-start(f32[16,1,384]{2,1,0:T(1,128)} %broadcast_in_dim.69), calls=%async_computation | async-start | bytes 49152 | tf_op jit(solution)/shard_map/all_to_all | solution.py:30
  71.2 4.5 %all-to-all-done = f32[16,1,384]{2,1,0:T(1,128)S(1)} async-done(((f32[16,1,384]{2,1,0:T(1,128)}), f32[16,1,384]{2,1,0:T(1,128)S(1)}, u32[]{:S(2)}, u32[]{:S(2)}) %all-to-all-start) | async-done | bytes 24608 | tf_op jit(solution)/shard_map/all_to_all | solution.py:30
  75.9 2.9 gather_fusion
  78.9 24.5 %all_to_all.35 = bf16[32,36,128]{2,1,0:T(8,128)(2,1)S(1)} all-to-all(bf16[32,36,128]{2,1,0:T(8,128)(2,1)S(1)} %all_to_all.24), channel_id=1, replica_groups=mesh['sp'=32,'tp'=16] {'sp'}, dimensions={0} | all-to-all | bytes 589824 | tf_op jit(solution)/shard_map/all_to_all | solution.py:129
  103.4 0.8 all_to_all.26
  104.2 45.8 %all-gather.5.cloned.1.call-done = bf16[1152,2048]{1,0:T(8,128)(2,1)} async-done(((bf16[1152,128]{1,0:T(8,128)(2,1)}), bf16[1152,2048]{1,0:T(8,128)(2,1)}) %all-gather.5.cloned.1.call-update) | async-done | bytes 4718608 | tf_op jit(solution)/shard_map/all_gather | solution.py:130
  150.0 3.9 fusion.7
  153.9 1.5 fusion
  155.8 4.9 %stack.2 = bf16[16,1152,256]{1,2,0:T(8,128)(2,1)} broadcast(bf16[1152,256]{0,1:T(8,128)(2,1)S(1)} %copy.41), dimensions={1,2} | broadcast | bytes 10027008 | tf_op jit(solution)/shard_map/stack | solution.py:141
  160.7 7.4 %all-to-all-start.2 = ((bf16[16,1152,256]{1,2,0:T(8,128)(2,1)}), bf16[16,1152,256]{1,2,0:T(8,128)(2,1)}, u32[]{:S(2)}, u32[]{:S(2)}) async-start(bf16[16,1152,256]{1,2,0:T(8,128)(2,1)} %stack.2), calls=%async_computation.2 | async-start | bytes 18874368 | tf_op jit(solution)/shard_map/all_to_all | solution.py:140
  168.1 206.1 %all-to-all-done.2 = bf16[16,1152,256]{1,2,0:T(8,128)(2,1)} async-done(((bf16[16,1152,256]{1,2,0:T(8,128)(2,1)}), bf16[16,1152,256]{1,2,0:T(8,128)(2,1)}, u32[]{:S(2)}, u32[]{:S(2)}) %all-to-all-start.2) | async-done | bytes 9437216 | tf_op jit(solution)/shard_map/all_to_all | solution.py:140
  374.2 6.4 %convolution_convert_fusion = bf16[1152,128]{1,0:T(8,128)(2,1)S(1)} fusion(bf16[1152,4096]{0,1:T(8,128)(2,1)} %bitcast.8, bf16[1,4096,128]{2,1,0:T(8,128)(2,1)S(1)} %copy-done.13), kind=kOutput, calls=%fused_computation.5 | convolution fusion | flops 1208107008 | bytes 10780672 | tf_op jit(solution)/shard_map/dot_general | solution.py:149
  380.5 0.8 all_to_all.28
  381.3 9.1 %all-to-all-start.3 = ((bf16[32,36,128]{2,1,0:T(8,128)(2,1)}), bf16[32,36,128]{2,1,0:T(8,128)(2,1)S(1)}, u32[]{:S(2)}, u32[]{:S(2)}) async-start(bf16[32,36,128]{2,1,0:T(8,128)(2,1)} %all_to_all.28), calls=%async_computation.3 | async-start | bytes 655360 | tf_op jit(solution)/shard_map/all_to_all | solution.py:152
  390.6 14.2 %all-to-all-done.3 = bf16[32,36,128]{2,1,0:T(8,128)(2,1)S(1)} async-done(((bf16[32,36,128]{2,1,0:T(8,128)(2,1)}), bf16[32,36,128]{2,1,0:T(8,128)(2,1)S(1)}, u32[]{:S(2)}, u32[]{:S(2)}) %all-to-all-start.3) | async-done | bytes 294944 | tf_op jit(solution)/shard_map/all_to_all | solution.py:152
  404.9 1.9 gather_fusion.1
  (76 shorter events, 7.1 us)
Async XLA Ops:
  6.5 143.5 %copy-start = (bf16[1,2048,256]{2,1,0:T(8,128)(2,1)S(1)}, bf16[1,2048,256]{2,1,0:T(8,128)(2,1)}, u32[]{:S(2)}) copy-start(bf16[1,2048,256]{2,1,0:T(8,128)(2,1)} %param.23) | copy-start | bytes 3145732
  6.5 7.1 %copy-start.5 = (bf16[64,384]{1,0:T(8,128)(2,1)S(1)}, bf16[64,384]{1,0:T(8,128)(2,1)}, u32[]{:S(2)}) copy-start(bf16[64,384]{1,0:T(8,128)(2,1)} %param.14) | copy-start | bytes 147460
  6.5 7.8 %copy-start.8 = (s32[384,2]{0,1:T(2,128)S(1)}, s32[384,2]{0,1:T(2,128)}, u32[]{:S(2)}) copy-start(s32[384,2]{0,1:T(2,128)} %param.20) | copy-start | bytes 9220
  6.5 55.2 %all-gather.3.cloned.1.call-start = ((), (), s32[]{:S(2)}) async-start(), calls=%async_computation.4 | async-start | bytes 1671168 | tf_op jit(solution)/shard_map/all_gather | solution.py:25
  7.4 4.8 %collective-permute-start = (bf16[64,15]{1,0:T(8,128)(2,1)S(1)}, bf16[64,15]{1,0:T(8,128)(2,1)S(1)}, u32[]{:S(2)}, u32[]{:S(2)}) collective-permute-start(bf16[64,15]{1,0:T(8,128)(2,1)S(1)} %slice.43), channel_id=1, source_target_pairs={{0,16},{16,32},{32,48},{48,64},{64,80},{80,96},{96,112},{112,128},... | collective-permute-start | bytes 5768 | tf_op jit(solution)/shard_map/ppermute | solution.py:16
  14.4 47.4 %copy-start.2 = (bf16[4,256,256]{2,1,0:T(8,128)(2,1)S(1)}, bf16[4,256,256]{2,1,0:T(8,128)(2,1)}, u32[]{:S(2)}) copy-start(bf16[4,256,256]{2,1,0:T(8,128)(2,1)} %param.15) | copy-start | bytes 1572868
  61.8 1.6 slice-start
  61.8 2.1 copy-start.1
  61.8 2.1 copy-start.9
  63.9 1.0 copy-start.3
  63.9 1.0 copy-start.4
  64.0 11.8 %copy-start.10 = (f32[128]{0:T(128)S(1)}, f32[128]{0:T(128)}, u32[]{:S(2)}) copy-start(f32[128]{0:T(128)} %param.19) | copy-start | bytes 1540
  66.0 9.7 %all-to-all-start = ((f32[16,1,384]{2,1,0:T(1,128)}), f32[16,1,384]{2,1,0:T(1,128)S(1)}, u32[]{:S(2)}, u32[]{:S(2)}) async-start(f32[16,1,384]{2,1,0:T(1,128)} %broadcast_in_dim.69), calls=%async_computation | async-start | bytes 49152 | tf_op jit(solution)/shard_map/all_to_all | solution.py:30
  71.1 78.9 %all-gather.5.cloned.1.call-start = ((), (), s32[]{:S(2)}) async-start(), calls=%async_computation.5 | async-start | bytes 5013504 | tf_op jit(solution)/shard_map/all_gather | solution.py:130
  104.2 49.8 %copy-start.12 = (bf16[1,2048,256]{2,1,0:T(8,128)(2,1)S(1)}, bf16[1,2048,256]{2,1,0:T(8,128)(2,1)}, u32[]{:S(2)}) copy-start(bf16[1,2048,256]{2,1,0:T(8,128)(2,1)} %param.24) | copy-start | bytes 3145732
  150.0 3.9 copy-start.11
  160.7 7.4 %copy-start.6 = (f32[384,4]{0,1:T(4,128)S(1)}, f32[384,4]{0,1:T(4,128)}, u32[]{:S(2)}) copy-start(f32[384,4]{0,1:T(4,128)} %param.21) | copy-start | bytes 18436
  160.7 213.5 %copy-start.13 = (bf16[1,4096,128]{2,1,0:T(8,128)(2,1)S(1)}, bf16[1,4096,128]{2,1,0:T(8,128)(2,1)}, u32[]{:S(2)}) copy-start(bf16[1,4096,128]{2,1,0:T(8,128)(2,1)} %param.25) | copy-start | bytes 3145732
  160.7 213.5 %all-to-all-start.2 = ((bf16[16,1152,256]{1,2,0:T(8,128)(2,1)}), bf16[16,1152,256]{1,2,0:T(8,128)(2,1)}, u32[]{:S(2)}, u32[]{:S(2)}) async-start(bf16[16,1152,256]{1,2,0:T(8,128)(2,1)} %stack.2), calls=%async_computation.2 | async-start | bytes 18874368 | tf_op jit(solution)/shard_map/all_to_all | solution.py:140
  374.2 16.2 %copy-start.7 = (f32[384,2]{0,1:T(2,128)S(1)}, f32[384,2]{0,1:T(2,128)}, u32[]{:S(2)}) copy-start(f32[384,2]{0,1:T(2,128)} %param.22) | copy-start | bytes 9220
  381.3 23.6 %all-to-all-start.3 = ((bf16[32,36,128]{2,1,0:T(8,128)(2,1)}), bf16[32,36,128]{2,1,0:T(8,128)(2,1)S(1)}, u32[]{:S(2)}, u32[]{:S(2)}) async-start(bf16[32,36,128]{2,1,0:T(8,128)(2,1)} %all_to_all.28), calls=%async_computation.3 | async-start | bytes 655360 | tf_op jit(solution)/shard_map/all_to_all | solution.py:152
Sparse Core Ops, SparseCore 0:
  14.5 47.2 all-gather.2
  104.3 45.6 all-gather.4
